TPU v7x, 32 devices: a whole 2x2x4 slice. The times are simulated.
32 devices in a mesh: grp: 2 (over y), sp: 4 (over z), tp: 4 (over x, core).
Axes of the slice: x: 2, y: 2, z: 4, core: 2. Of those that a mesh axis runs over, the one named last changes fastest.
Arguments:
- tokens: bfloat16 [1024, 2048], P(('grp', 'sp')), parts along dimension 0, may hold values from -8 to 8
- norm_gain: float32 [2048], replicated, may hold values from 0.1 to 1.9
- w_query: bfloat16 [2048, 1024], P(None, 'tp'), may hold values from -0.125 to 0.125
- w_key: bfloat16 [2048, 1024], P(None, 'tp'), may hold values from -0.125 to 0.125
- w_value: bfloat16 [2048, 1024], P(None, 'tp'), may hold values from -0.125 to 0.125
- w_out: bfloat16 [1024, 2048], P('tp'), may hold values from -0.1875 to 0.1875
- key_rate: bfloat16 [16, 1024], P('tp', ('grp', 'sp')), parts along dimension 1, may hold values from -16 to 1
Outputs:
- layer_out: bfloat16 [1024, 2048], P(('grp', 'sp')), parts along dimension 0
There are 2 independent parts, one for each index of `grp`. A program takes and returns all parts, laid end to end along the dimension named above; an argument that names none is the same for every part. Nothing has to cross between parts.
All inputs are finite; a program needn't handle non-finite values.
Results may differ from a plain program's by a relative error of at most 0.0075.
Values may be sent and summed in bfloat16 or wider, within the bound.
No kernel may reach another device: no remote copies, remote signals or barrier semaphores. Data moves between devices by JAX's collectives and lax.ppermute only.
A program may use at most 64 MiB of HBM per device.

v0:
```python
import jax
import jax.numpy as jnp
from jax import lax
from jax.sharding import PartitionSpec as P

HD = 64
KEY_SPAN = 128
F32 = jnp.float32
BF16 = jnp.bfloat16
HIGHEST = lax.Precision.HIGHEST
EPS = 1e-06


def break_scores(query_heads, key_heads, rate_row_values, query_pos, key_pos):
    scores = jnp.einsum(
        "qhd,khd->hqk", query_heads, key_heads, preferred_element_type=F32
    ) * HD ** (-0.5)
    scores = scores + jnp.transpose(rate_row_values).astype(F32)[:, None, :]
    causal_mask = key_pos[None, :] < query_pos[:, None]
    log_remain = jnp.where(causal_mask[None], jax.nn.log_sigmoid(-scores), 0.0)
    return (scores, causal_mask, log_remain)


def shard_summary(query_heads, key_heads, value_heads, rate_row_values, query_pos, key_pos):
    scores, causal_mask, log_remain = break_scores(
        query_heads, key_heads, rate_row_values, query_pos, key_pos
    )
    heads_here, query_count, key_count = scores.shape
    span_count = key_count // KEY_SPAN
    blocks = log_remain.reshape(heads_here, query_count, span_count, KEY_SPAN)
    span_ids = jnp.arange(KEY_SPAN, dtype=jnp.int32)
    tri_strict = (span_ids[:, None] > span_ids[None, :]).astype(F32)
    inside_sum = jnp.einsum("hqnj,js->hqns", blocks, tri_strict, precision=HIGHEST)
    block_ids = jnp.arange(span_count, dtype=jnp.int32)
    block_later = (block_ids[:, None] > block_ids[None, :]).astype(F32)
    beyond = jnp.einsum("hqn,nm->hqm", jnp.sum(blocks, axis=-1), block_later, precision=HIGHEST)
    suffix = (inside_sum + beyond[..., None]).reshape(heads_here, query_count, key_count)
    weight = jnp.where(causal_mask[None], jnp.exp(jax.nn.log_sigmoid(scores) + suffix), 0.0).astype(
        BF16
    )
    partial_value = jnp.einsum("hqk,khd->qhd", weight, value_heads, preferred_element_type=F32)
    return (partial_value.reshape(query_count, heads_here * HD), jnp.sum(log_remain, axis=-1))


def on_device(tokens, norm_gain, w_query, w_key, w_value, w_out, key_rate):
    tokens_f = tokens.astype(F32)
    normed = (
        tokens_f
        * lax.rsqrt(jnp.mean(tokens_f * tokens_f, axis=-1, keepdims=True) + EPS)
        * norm_gain
    ).astype(BF16)
    queries = jnp.dot(normed, w_query, preferred_element_type=F32).astype(BF16)
    key_rows = jnp.dot(normed, w_key, preferred_element_type=F32).astype(BF16)
    value_rows = jnp.dot(normed, w_value, preferred_element_type=F32).astype(BF16)
    head_width = w_query.shape[1]
    heads_local = head_width // HD
    row_count = tokens.shape[0]
    rate_row_values = jnp.transpose(key_rate)
    query_heads = queries.reshape(row_count, heads_local, HD)
    own_shard = lax.axis_index("sp")
    shard_total = lax.axis_size("sp")
    local_pos = jnp.arange(row_count, dtype=jnp.int32)
    shard_ids = jnp.arange(shard_total, dtype=jnp.int32)
    later_mask = (shard_ids[:, None] > shard_ids[None, :]).astype(F32)
    query_groups = [(query_heads, own_shard * row_count)]

    def summarize(key_block, value_block, rate_block, first_key):
        key_pos = first_key + local_pos
        group_heads, group_start = query_groups[0]
        group_count = group_heads.shape[0]
        group_pos = group_start + jnp.arange(group_count, dtype=jnp.int32)
        empty_pair = (
            jnp.zeros((group_count, head_width), F32),
            jnp.zeros((heads_local, group_count), F32),
        )
        partial_value, remain = lax.cond(
            first_key < group_start + group_count - 1,
            lambda: shard_summary(
                group_heads, key_block, value_block, rate_block, group_pos, key_pos
            ),
            lambda: empty_pair,
        )
        partial_list = [partial_value]
        remain_list = [remain]
        return (jnp.concatenate(partial_list, axis=0), jnp.concatenate(remain_list, axis=1))

    initial = (
        jnp.zeros((shard_total, row_count, head_width), F32),
        jnp.zeros((shard_total, heads_local, row_count), F32),
    )
    piece_keys = lax.all_gather(key_rows, "sp", axis=0, tiled=True)
    piece_values = lax.all_gather(value_rows, "sp", axis=0, tiled=True)
    piece_rates = lax.all_gather(rate_row_values, "sp", axis=0, tiled=True)
    piece_count = piece_keys.shape[0] // row_count
    key_blocks = piece_keys.reshape(piece_count, row_count, heads_local, HD)
    value_blocks = piece_values.reshape(piece_count, row_count, heads_local, HD)
    rate_blocks = piece_rates.reshape(piece_count, row_count, heads_local)

    def absorb_one(inner_pair, item_tuple):
        item_index, key_block, value_block, rate_block = item_tuple
        first_key = item_index * row_count
        shard_index = first_key // row_count
        partial_value, remain = summarize(key_block, value_block, rate_block, first_key)
        partials = lax.dynamic_update_index_in_dim(inner_pair[0], partial_value, shard_index, 0)
        remains = lax.dynamic_update_index_in_dim(inner_pair[1], remain, shard_index, 0)
        return ((partials, remains), None)

    result, _ = lax.scan(
        absorb_one,
        initial,
        (jnp.arange(piece_count, dtype=jnp.int32), key_blocks, value_blocks, rate_blocks),
    )
    partials, remains = result
    beyond = jnp.einsum("nhq,nm->mhq", remains, later_mask, precision=HIGHEST)
    factor = jnp.transpose(jnp.exp(beyond), (0, 2, 1))[..., None]
    mixed_rows = jnp.sum(partials.reshape(shard_total, row_count, heads_local, HD) * factor, axis=0)
    mixed = mixed_rows.reshape(row_count, head_width).astype(BF16)
    token_heads = lax.all_to_all(mixed, "tp", split_axis=0, concat_axis=1, tiled=True)
    whole_out = lax.all_gather(w_out, "tp", axis=0, tiled=True)
    own_rows = jnp.dot(token_heads, whole_out, preferred_element_type=F32).astype(BF16)
    return lax.all_gather(own_rows, "tp", axis=0, tiled=True)


def solution(mesh):
    return jax.shard_map(
        on_device,
        mesh=mesh,
        in_specs=(
            P(("grp", "sp"), None),
            P(),
            P(None, "tp"),
            P(None, "tp"),
            P(None, "tp"),
            P("tp", None),
            P("tp", ("grp", "sp")),
        ),
        out_specs=P(("grp", "sp"), None),
        check_vma=False,
    )
```

profile of v0, /device:TPU:25, one launch (start us, length us, event | category | flops | bytes accessed | tf_op | source)
XLA Modules:
  0.0 93.3 jit_solution(17264272396755167459)
XLA Ops:
  7.3 1.2 %fusion.25 = f32[128]{0:T(128)S(1)} fusion(bf16[128,2048]{1,0:T(8,128)(2,1)} %param.11), kind=kLoop, calls=%fused_computation.40 | loop fusion | flops 786304 | bytes 524800 | tf_op jit(solution)/shard_map/reduce_sum | solution.py:49
  8.5 1.4 %convolution_convert_fusion.3 = bf16[128,256]{1,0:T(8,128)(2,1)S(1)} fusion(bf16[2048,256]{1,0:T(8,128)(2,1)S(1)} %copy-done, bf16[128,2048]{1,0:T(8,128)(2,1)} %param.11, f32[2048]{0:T(1024)} %param.12, f32[128]{0:T(128)S(1)} %add_rsqrt_fusion), kind=kOutput, calls=%fused_computation.37 | convolution fusion | flops 135299072 | bytes 1647104 | tf_op jit(solution)/shard_map/dot_general | solution.py:53
  9.9 11.0 %all_gather.15 = bf16[512,256]{1,0:T(8,128)(2,1)S(1)} all-gather(bf16[128,256]{1,0:T(8,128)(2,1)S(1)} %convolution_convert_fusion.3), channel_id=1, replica_groups=mesh['grp'=2,'sp'=4,'tp'=4] {'sp'}, dimensions={0}, use_global_device_ids=true | all-gather | bytes 327680 | tf_op jit(solution)/shard_map/all_gather | solution.py:91
  21.5 1.6 %convolution_convert_fusion.1 = bf16[128,256]{1,0:T(8,128)(2,1)S(1)} fusion(bf16[2048,256]{1,0:T(8,128)(2,1)} %param.15, bf16[128,2048]{1,0:T(8,128)(2,1)S(1)} %copy-done.1, f32[2048]{0:T(1024)S(1)} %copy-done.3, f32[128]{0:T(128)S(1)} %add_rsqrt_fusion), kind=kOutput, calls=%fused_computation.35 | convolution fusion | flops 135299072 | bytes 1647104 | tf_op jit(solution)/shard_map/dot_general | solution.py:54
  23.1 12.0 %all_gather.17 = bf16[512,256]{1,0:T(8,128)(2,1)S(1)} all-gather(bf16[128,256]{1,0:T(8,128)(2,1)S(1)} %convolution_convert_fusion.1), channel_id=1, replica_groups=mesh['grp'=2,'sp'=4,'tp'=4] {'sp'}, dimensions={0}, use_global_device_ids=true | all-gather | bytes 327680 | tf_op jit(solution)/shard_map/all_gather | solution.py:92
  35.6 1.6 %convolution_convert_fusion.2 = bf16[128,256]{1,0:T(8,128)(2,1)S(1)} fusion(bf16[2048,256]{1,0:T(8,128)(2,1)} %param.13, bf16[128,2048]{1,0:T(8,128)(2,1)S(1)} %copy-done.1, f32[2048]{0:T(1024)S(1)} %copy-done.3, f32[128]{0:T(128)S(1)} %add_rsqrt_fusion), kind=kOutput, calls=%fused_computation.36 | convolution fusion | flops 135299072 | bytes 1647104 | tf_op jit(solution)/shard_map/dot_general | solution.py:52
  37.3 5.6 %all_gather.16 = bf16[512,4]{0,1:T(4,128)(2,1)S(1)} all-gather(bf16[128,4]{0,1:T(4,128)(2,1)S(1)} %bitcast.58), channel_id=1, replica_groups=mesh['grp'=2,'sp'=4,'tp'=4] {'sp'}, dimensions={0}, use_global_device_ids=true | all-gather | bytes 5120 | tf_op jit(solution)/shard_map/all_gather | solution.py:93
  43.0 18.4 %while.16 = (s32[]{:T(128)}, f32[4,128,256]{1,2,0:T(8,128)S(1)}, f32[4,4,128]{2,0,1:T(4,128)S(1)}, s32[4]{0:T(128)S(1)}, s32[]{:T(128)}, /*index=5*/s32[]{:T(128...) while((s32[]{:T(128)}, f32[4,128,256]{1,2,0:T(8,128)S(1)}, ...), condition=%wide.region_5.6_spmd.clone, body=%wide.region_1.5_spmd.clone.sunk | while | flops 119505664 | bytes 1446895 | solution.py:108
  44.3 2.6 %conditional.3 = (f32[1,128,256]{1,2,0:T(8,128)S(1)}, f32[1,4,128]{2,1,0:T(4,128)}) conditional(s32[]{:T(128)} %convert_element_type.82, () %tuple.61, (s32[]{:T(128)}, s32[128]{0:T(128)S(1)}, s32[]{:T(128)}, s32[128]{0:T(128)S(1)}, bf16[4,128,4,64]{1,3,2,0:T(8,128)(2,1)S(1)}, /*index=5*/s32[]{:T(128)}, bf16[128,4,64]{0,2,1:T(8,128)(2,1)S(1)}, ...), branch_computations={%region_2.2_spmd, %region_3.4_spmd} | conditional | flops 119505664 | bytes 1179684 | solution.py:76
  44.4 1.0 %fusion.11 = (f32[4,128]{1,0:T(4,128)}, f32[4,128,128]{1,2,0:T(8,128)S(1)}) fusion(pred[128,128]{0,1:T(8,128)(4,1)S(1)} %broadcast_compare_fusion, f32[4,128]{1,0:T(4,128)S(1)} %convert_bitcast_fusion, bf16[128,4,64]{0,2,1:T(8,128)(2,1)S(1)} %get-tuple-element.246, bf16[4,128,4,64]{1,3,2,0:T(8,128)(2,1)S(1)} %get-tuple-element.244, s32[]{:T(128)} %get-tuple-element.245), kind=kOutput, calls=%fused_computation.14 | convolution fusion | flops 9108992 | bytes 413700 | tf_op jit(solution)/shard_map/while/body/eval_jaxpr/cond/branch_1_fun/qhd,khd->hqk/dot_general | solution.py:15
  46.9 0.7 dynamic_update_slice.22
  48.9 2.6 %conditional.3 = (f32[1,128,256]{1,2,0:T(8,128)S(1)}, f32[1,4,128]{2,1,0:T(4,128)}) conditional(s32[]{:T(128)} %convert_element_type.82, () %tuple.61, (s32[]{:T(128)}, s32[128]{0:T(128)S(1)}, s32[]{:T(128)}, s32[128]{0:T(128)S(1)}, bf16[4,128,4,64]{1,3,2,0:T(8,128)(2,1)S(1)}, /*index=5*/s32[]{:T(128)}, bf16[128,4,64]{0,2,1:T(8,128)(2,1)S(1)}, ...), branch_computations={%region_2.2_spmd, %region_3.4_spmd} | conditional | flops 119505664 | bytes 1179684 | solution.py:76
  49.0 1.0 %fusion.11 = (f32[4,128]{1,0:T(4,128)}, f32[4,128,128]{1,2,0:T(8,128)S(1)}) fusion(pred[128,128]{0,1:T(8,128)(4,1)S(1)} %broadcast_compare_fusion, f32[4,128]{1,0:T(4,128)S(1)} %convert_bitcast_fusion, bf16[128,4,64]{0,2,1:T(8,128)(2,1)S(1)} %get-tuple-element.246, bf16[4,128,4,64]{1,3,2,0:T(8,128)(2,1)S(1)} %get-tuple-element.244, s32[]{:T(128)} %get-tuple-element.245), kind=kOutput, calls=%fused_computation.14 | convolution fusion | flops 9108992 | bytes 413700 | tf_op jit(solution)/shard_map/while/body/eval_jaxpr/cond/branch_1_fun/qhd,khd->hqk/dot_general | solution.py:15
  51.5 0.7 dynamic_update_slice.22
  53.5 2.6 %conditional.3 = (f32[1,128,256]{1,2,0:T(8,128)S(1)}, f32[1,4,128]{2,1,0:T(4,128)}) conditional(s32[]{:T(128)} %convert_element_type.82, () %tuple.61, (s32[]{:T(128)}, s32[128]{0:T(128)S(1)}, s32[]{:T(128)}, s32[128]{0:T(128)S(1)}, bf16[4,128,4,64]{1,3,2,0:T(8,128)(2,1)S(1)}, /*index=5*/s32[]{:T(128)}, bf16[128,4,64]{0,2,1:T(8,128)(2,1)S(1)}, ...), branch_computations={%region_2.2_spmd, %region_3.4_spmd} | conditional | flops 119505664 | bytes 1179684 | solution.py:76
  53.6 1.0 %fusion.11 = (f32[4,128]{1,0:T(4,128)}, f32[4,128,128]{1,2,0:T(8,128)S(1)}) fusion(pred[128,128]{0,1:T(8,128)(4,1)S(1)} %broadcast_compare_fusion, f32[4,128]{1,0:T(4,128)S(1)} %convert_bitcast_fusion, bf16[128,4,64]{0,2,1:T(8,128)(2,1)S(1)} %get-tuple-element.246, bf16[4,128,4,64]{1,3,2,0:T(8,128)(2,1)S(1)} %get-tuple-element.244, s32[]{:T(128)} %get-tuple-element.245), kind=kOutput, calls=%fused_computation.14 | convolution fusion | flops 9108992 | bytes 413700 | tf_op jit(solution)/shard_map/while/body/eval_jaxpr/cond/branch_1_fun/qhd,khd->hqk/dot_general | solution.py:15
  56.1 0.7 dynamic_update_slice.22
  58.1 2.6 %conditional.3 = (f32[1,128,256]{1,2,0:T(8,128)S(1)}, f32[1,4,128]{2,1,0:T(4,128)}) conditional(s32[]{:T(128)} %convert_element_type.82, () %tuple.61, (s32[]{:T(128)}, s32[128]{0:T(128)S(1)}, s32[]{:T(128)}, s32[128]{0:T(128)S(1)}, bf16[4,128,4,64]{1,3,2,0:T(8,128)(2,1)S(1)}, /*index=5*/s32[]{:T(128)}, bf16[128,4,64]{0,2,1:T(8,128)(2,1)S(1)}, ...), branch_computations={%region_2.2_spmd, %region_3.4_spmd} | conditional | flops 119505664 | bytes 1179684 | solution.py:76
  58.2 1.0 %fusion.11 = (f32[4,128]{1,0:T(4,128)}, f32[4,128,128]{1,2,0:T(8,128)S(1)}) fusion(pred[128,128]{0,1:T(8,128)(4,1)S(1)} %broadcast_compare_fusion, f32[4,128]{1,0:T(4,128)S(1)} %convert_bitcast_fusion, bf16[128,4,64]{0,2,1:T(8,128)(2,1)S(1)} %get-tuple-element.246, bf16[4,128,4,64]{1,3,2,0:T(8,128)(2,1)S(1)} %get-tuple-element.244, s32[]{:T(128)} %get-tuple-element.245), kind=kOutput, calls=%fused_computation.14 | convolution fusion | flops 9108992 | bytes 413700 | tf_op jit(solution)/shard_map/while/body/eval_jaxpr/cond/branch_1_fun/qhd,khd->hqk/dot_general | solution.py:15
  60.7 0.7 dynamic_update_slice.22
  61.7 13.7 %all_to_all.16 = bf16[4,32,256]{2,1,0:T(8,128)(2,1)S(1)} all-to-all(bf16[4,32,256]{2,1,0:T(8,128)(2,1)S(1)} %bitcast.54), channel_id=1, replica_groups=mesh['grp'=2,'sp'=4,'tp'=4] {'tp'}, dimensions={0} | all-to-all | bytes 131072 | tf_op jit(solution)/shard_map/all_to_all | solution.py:118
  75.4 3.0 %convolution_convert_fusion = bf16[32,2048]{1,0:T(8,128)(2,1)S(1)} fusion(bf16[32,1024]{1,0:T(8,128)(2,1)S(1)} %bitcast.53, bf16[1024,2048]{1,0:T(8,128)(2,1)} %all-gather.2.cloned.1.call-done), kind=kOutput, calls=%fused_computation.32 | convolution fusion | flops 134283264 | bytes 4390912 | tf_op jit(solution)/shard_map/dot_general | solution.py:120
  78.4 7.3 %all_gather.19 = bf16[128,2048]{1,0:T(8,128)(2,1)S(1)} all-gather(bf16[32,2048]{1,0:T(8,128)(2,1)S(1)} %convolution_convert_fusion), channel_id=1, replica_groups=mesh['grp'=2,'sp'=4,'tp'=4] {'tp'}, dimensions={0}, use_global_device_ids=true | all-gather | bytes 655360 | tf_op jit(solution)/shard_map/all_gather | solution.py:121
  85.7 0.8 copy.73
  (61 shorter events, 10.8 us)
Async XLA Ops:
  6.5 2.0 %copy-start = (bf16[2048,256]{1,0:T(8,128)(2,1)S(1)}, bf16[2048,256]{1,0:T(8,128)(2,1)}, u32[]{:S(2)}) copy-start(bf16[2048,256]{1,0:T(8,128)(2,1)} %param.14) | copy-start | bytes 3145732
  6.5 14.9 %copy-start.1 = (bf16[128,2048]{1,0:T(8,128)(2,1)S(1)}, bf16[128,2048]{1,0:T(8,128)(2,1)}, u32[]{:S(2)}) copy-start(bf16[128,2048]{1,0:T(8,128)(2,1)} %param.11) | copy-start | bytes 1572868
  6.5 14.9 %copy-start.3 = (f32[2048]{0:T(1024)S(1)}, f32[2048]{0:T(1024)}, u32[]{:S(2)}) copy-start(f32[2048]{0:T(1024)} %param.12) | copy-start | bytes 24580
  6.5 68.8 %all-gather.2.cloned.1.call-start = ((), (), s32[]{:S(2)}) async-start(), calls=%async_computation.1 | async-start | bytes 5242880 | tf_op jit(solution)/shard_map/all_gather | solution.py:119
  9.9 27.4 %copy-start.2 = (bf16[4,128]{1,0:T(4,128)(2,1)S(1)}, bf16[4,128]{1,0:T(4,128)(2,1)}, u32[]{:S(2)}) copy-start(bf16[4,128]{1,0:T(4,128)(2,1)} %param.17) | copy-start | bytes 3076
Sparse Core Ops, SparseCore 0:
  8.9 35.8 all-gather.1
where the time goes:
time: 93.8 us; the launch traced here: 93.3 us
  blocking collectives  49.5 us (53%)
  matrix products  14.6 us (16%)
  between operations  13.5 us (14%)
  local copies, waits for them, and re-layouts  7.46 us (8%)
  other arithmetic  4.42 us (5%)
  loops' own time  3.02 us (3%)
    all_to_all x1, blocking collectives, on_device(): lax.all_to_all(mixed, 'tp', split_axis=0, concat_axis=1, tiled=True)  13.7 us
    all_gather x1, blocking collectives, on_device(): piece_values = lax.all_gather(value_rows, 'sp', axis=0, tiled=True)  12 us
    all_gather x1, blocking collectives, on_device(): piece_keys = lax.all_gather(key_rows, 'sp', axis=0, tiled=True)  11 us
    all_gather x1, blocking collectives, on_device(): return lax.all_gather(own_rows, 'tp', axis=0, tiled=True)  7.28 us
    all_gather x1, blocking collectives, on_device(): piece_rates = lax.all_gather(rate_row_values, 'sp', axis=0, tiled=True)  5.6 us
    dot_general x4, matrix products, break_scores(): jnp.einsum('qhd,khd->hqk', query_heads, key_heads, preferred_element_type...  3.93 us
    dot_general x1, matrix products, on_device(): jnp.dot(token_heads, whole_out, preferred_element_type=F32).astype(BF16)  3.01 us
    dynamic_update_slice x4, local copies, waits for them, and re-layouts, absorb_one(): lax.dynamic_update_index_in_dim(inner_pair[1], remain, shard_index, 0)  2.88 us
  transfers between devices with their start and end apart: 1, of which 0 were waited for; matrix products, arithmetic and copies ran while one was open for 24% of the time, Pallas kernels for 0%

commit v1 on v0

--- a/solution.py
+++ b/solution.py
@@ -88,7 +88,12 @@
         jnp.zeros((shard_total, row_count, head_width), F32),
         jnp.zeros((shard_total, heads_local, row_count), F32),
     )
-    piece_keys = lax.all_gather(key_rows, "sp", axis=0, tiled=True)
+    ring = [key_rows]
+    for hop in range(3):
+        ring.append(lax.ppermute(ring[-1], "sp", [(dev, (dev + 1) % 4) for dev in range(4)]))
+    piece_keys = jnp.roll(
+        jnp.concatenate(ring[::-1], axis=0), (lax.axis_index("sp") + 1) * ring[0].shape[0], axis=0
+    )
     piece_values = lax.all_gather(value_rows, "sp", axis=0, tiled=True)
     piece_rates = lax.all_gather(rate_row_values, "sp", axis=0, tiled=True)
     piece_count = piece_keys.shape[0] // row_count

time: 93.8 us -> 88.6 us (0.945)
  blocking collectives: 49.5 us -> 37.5 us
  starting transfers between devices: 0.01 us -> 5.48 us
  waiting for transfers between devices: 0.71 us -> 2.96 us
  matrix products: 14.6 us -> 13.6 us
    all_gather x1 -> x0, blocking collectives: 11 us -> none  [on_device(): piece_keys = lax.all_gather(key_rows, 'sp', axis=0, tiled=True)]
    ppermute x0 -> x3, starting transfers between devices: none -> 5.44 us  [on_device(): lax.ppermute(ring[-1], 'sp', [(dev, (dev + 1) % 4) for dev in range(4)])]
    ppermute x0 -> x3, waiting for transfers between devices: none -> 2.28 us  [on_device(): lax.ppermute(ring[-1], 'sp', [(dev, (dev + 1) % 4) for dev in range(4)])]
    dot_general x1, matrix products: 1.58 us -> 0.36 us  [on_device(): queries = jnp.dot(normed, w_query, preferred_element_type=F32).astype(BF16)]
  transfers between devices with their start and end apart: 1 -> 4, of which waited for: 0 -> 2; matrix products, arithmetic and copies ran while one was open for 24% -> 25% of each run, Pallas kernels for 0% -> 0%
where the time goes in v1:
time: 88.6 us; the launch traced here: 88.2 us
  blocking collectives  37.5 us (42%)
  matrix products  13.6 us (15%)
  between operations  13.6 us (15%)
  local copies, waits for them, and re-layouts  7.5 us (8%)
  starting transfers between devices  5.48 us (6%)
  other arithmetic  4.48 us (5%)
  loops' own time  3.02 us (3%)
  waiting for transfers between devices  2.96 us (3%)
    all_to_all x1, blocking collectives, on_device(): lax.all_to_all(mixed, 'tp', split_axis=0, concat_axis=1, tiled=True)  13.2 us
    all_gather x1, blocking collectives, on_device(): piece_values = lax.all_gather(value_rows, 'sp', axis=0, tiled=True)  11.5 us
    all_gather x1, blocking collectives, on_device(): return lax.all_gather(own_rows, 'tp', axis=0, tiled=True)  7.28 us
    all_gather x1, blocking collectives, on_device(): piece_rates = lax.all_gather(rate_row_values, 'sp', axis=0, tiled=True)  5.6 us
    ppermute x3, starting transfers between devices, on_device(): lax.ppermute(ring[-1], 'sp', [(dev, (dev + 1) % 4) for dev in range(4)])  5.44 us
    dot_general x4, matrix products, break_scores(): jnp.einsum('qhd,khd->hqk', query_heads, key_heads, preferred_element_type...  3.93 us
    dot_general x1, matrix products, on_device(): jnp.dot(token_heads, whole_out, preferred_element_type=F32).astype(BF16)  3.01 us
    dynamic_update_slice x4, local copies, waits for them, and re-layouts, absorb_one(): lax.dynamic_update_index_in_dim(inner_pair[1], remain, shard_index, 0)  2.88 us
  transfers between devices with their start and end apart: 4, of which 2 were waited for; matrix products, arithmetic and copies ran while one was open for 25% of the time, Pallas kernels for 0%

profile of v1, /device:TPU:25, one launch (start us, length us, event | category | flops | bytes accessed | tf_op | source)
XLA Modules:
  0.0 88.2 jit_solution(2794309531280793079)
XLA Ops:
  7.3 1.3 %fusion.25 = f32[128]{0:T(128)S(1)} fusion(bf16[128,2048]{1,0:T(8,128)(2,1)} %param.11), kind=kLoop, calls=%fused_computation.40 | loop fusion | flops 786304 | bytes 524800 | tf_op jit(solution)/shard_map/reduce_sum | solution.py:49
  8.6 1.4 %convolution_convert_fusion.3 = bf16[128,256]{1,0:T(8,128)(2,1)S(1)} fusion(bf16[2048,256]{1,0:T(8,128)(2,1)S(1)} %copy-done, bf16[128,2048]{1,0:T(8,128)(2,1)} %param.11, f32[2048]{0:T(1024)} %param.12, f32[128]{0:T(128)S(1)} %add_rsqrt_fusion), kind=kOutput, calls=%fused_computation.37 | convolution fusion | flops 135299072 | bytes 1647104 | tf_op jit(solution)/shard_map/dot_general | solution.py:53
  10.1 1.8 %convolution_convert_fusion.1 = bf16[128,256]{1,0:T(8,128)(2,1)S(1)} fusion(bf16[2048,256]{1,0:T(8,128)(2,1)} %param.15, bf16[128,2048]{1,0:T(8,128)(2,1)} %param.11, f32[2048]{0:T(1024)} %param.12, f32[128]{0:T(128)S(1)} %add_rsqrt_fusion), kind=kOutput, calls=%fused_computation.35 | convolution fusion | flops 135299072 | bytes 1647104 | tf_op jit(solution)/shard_map/dot_general | solution.py:54
  11.8 1.3 %collective-permute-done = bf16[128,256]{1,0:T(8,128)(2,1)S(1)} collective-permute-done((bf16[128,256]{1,0:T(8,128)(2,1)S(1)}, bf16[128,256]{1,0:T(8,128)(2,1)S(1)}, u32[]{:S(2)}, u32[]{:S(2)}) %collective-permute-start) | collective-permute-done | bytes 65568 | tf_op jit(solution)/shard_map/ppermute | solution.py:93
  13.2 1.8 %collective-permute-start.1 = (bf16[128,256]{1,0:T(8,128)(2,1)S(1)}, bf16[128,256]{1,0:T(8,128)(2,1)S(1)}, u32[]{:S(2)}, u32[]{:S(2)}) collective-permute-start(bf16[128,256]{1,0:T(8,128)(2,1)S(1)} %collective-permute-done), channel_id=1, source_target_pairs={{0,4},{4,8},{8,12},{12,0},{1,5},{5,9},{9,13},{13,1},{2,6},{6,10},{... | collective-permute-start | bytes 196616 | tf_op jit(solution)/shard_map/ppermute | solution.py:93
  15.4 0.9 %collective-permute-done.1 = bf16[128,256]{1,0:T(8,128)(2,1)S(1)} collective-permute-done((bf16[128,256]{1,0:T(8,128)(2,1)S(1)}, bf16[128,256]{1,0:T(8,128)(2,1)S(1)}, u32[]{:S(2)}, u32[]{:S(2)}) %collective-permute-start.1) | collective-permute-done | bytes 65568 | tf_op jit(solution)/shard_map/ppermute | solution.py:93
  16.3 3.6 %collective-permute-start.2 = (bf16[128,256]{1,0:T(8,128)(2,1)S(1)}, bf16[128,256]{1,0:T(8,128)(2,1)S(1)}, u32[]{:S(2)}, u32[]{:S(2)}) collective-permute-start(bf16[128,256]{1,0:T(8,128)(2,1)S(1)} %collective-permute-done.1), channel_id=1, source_target_pairs={{0,4},{4,8},{8,12},{12,0},{1,5},{5,9},{9,13},{13,1},{2,6},{6,10},{... | collective-permute-start | bytes 196616 | tf_op jit(solution)/shard_map/ppermute | solution.py:93
  19.9 11.5 %all_gather.13 = bf16[512,256]{1,0:T(8,128)(2,1)S(1)} all-gather(bf16[128,256]{1,0:T(8,128)(2,1)S(1)} %convolution_convert_fusion.1), channel_id=1, replica_groups=mesh['grp'=2,'sp'=4,'tp'=4] {'sp'}, dimensions={0}, use_global_device_ids=true | all-gather | bytes 327680 | tf_op jit(solution)/shard_map/all_gather | solution.py:97
  32.0 5.6 %all_gather.12 = bf16[512,4]{0,1:T(4,128)(2,1)S(1)} all-gather(bf16[128,4]{0,1:T(4,128)(2,1)S(1)} %bitcast.58), channel_id=1, replica_groups=mesh['grp'=2,'sp'=4,'tp'=4] {'sp'}, dimensions={0}, use_global_device_ids=true | all-gather | bytes 5120 | tf_op jit(solution)/shard_map/all_gather | solution.py:98
  38.4 18.4 %while.16 = (s32[]{:T(128)}, f32[4,128,256]{1,2,0:T(8,128)S(1)}, f32[4,4,128]{2,0,1:T(4,128)S(1)}, s32[4]{0:T(128)S(1)}, s32[]{:T(128)}, /*index=5*/s32[]{:T(128...) while((s32[]{:T(128)}, f32[4,128,256]{1,2,0:T(8,128)S(1)}, ...), condition=%wide.region_5.6_spmd.clone, body=%wide.region_1.5_spmd.clone.sunk | while | flops 119505664 | bytes 1446895 | solution.py:113
  39.6 2.6 %conditional.3 = (f32[1,128,256]{1,2,0:T(8,128)S(1)}, f32[1,4,128]{2,1,0:T(4,128)}) conditional(s32[]{:T(128)} %convert_element_type.82, () %tuple.61, (s32[]{:T(128)}, s32[128]{0:T(128)S(1)}, s32[]{:T(128)}, s32[128]{0:T(128)S(1)}, bf16[4,128,4,64]{1,3,2,0:T(8,128)(2,1)S(1)}, /*index=5*/s32[]{:T(128)}, bf16[128,4,64]{0,2,1:T(8,128)(2,1)S(1)}, ...), branch_computations={%region_2.2_spmd, %region_3.4_spmd} | conditional | flops 119505664 | bytes 1179684 | solution.py:76
  39.8 1.0 %fusion.11 = (f32[4,128]{1,0:T(4,128)}, f32[4,128,128]{1,2,0:T(8,128)S(1)}) fusion(pred[128,128]{0,1:T(8,128)(4,1)S(1)} %broadcast_compare_fusion, f32[4,128]{1,0:T(4,128)S(1)} %convert_bitcast_fusion, bf16[128,4,64]{0,2,1:T(8,128)(2,1)S(1)} %get-tuple-element.246, bf16[4,128,4,64]{1,3,2,0:T(8,128)(2,1)S(1)} %get-tuple-element.244, s32[]{:T(128)} %get-tuple-element.245), kind=kOutput, calls=%fused_computation.14 | convolution fusion | flops 9108992 | bytes 413700 | tf_op jit(solution)/shard_map/while/body/eval_jaxpr/cond/branch_1_fun/qhd,khd->hqk/dot_general | solution.py:15
  42.2 0.7 dynamic_update_slice.22
  44.3 2.6 %conditional.3 = (f32[1,128,256]{1,2,0:T(8,128)S(1)}, f32[1,4,128]{2,1,0:T(4,128)}) conditional(s32[]{:T(128)} %convert_element_type.82, () %tuple.61, (s32[]{:T(128)}, s32[128]{0:T(128)S(1)}, s32[]{:T(128)}, s32[128]{0:T(128)S(1)}, bf16[4,128,4,64]{1,3,2,0:T(8,128)(2,1)S(1)}, /*index=5*/s32[]{:T(128)}, bf16[128,4,64]{0,2,1:T(8,128)(2,1)S(1)}, ...), branch_computations={%region_2.2_spmd, %region_3.4_spmd} | conditional | flops 119505664 | bytes 1179684 | solution.py:76
  44.4 1.0 %fusion.11 = (f32[4,128]{1,0:T(4,128)}, f32[4,128,128]{1,2,0:T(8,128)S(1)}) fusion(pred[128,128]{0,1:T(8,128)(4,1)S(1)} %broadcast_compare_fusion, f32[4,128]{1,0:T(4,128)S(1)} %convert_bitcast_fusion, bf16[128,4,64]{0,2,1:T(8,128)(2,1)S(1)} %get-tuple-element.246, bf16[4,128,4,64]{1,3,2,0:T(8,128)(2,1)S(1)} %get-tuple-element.244, s32[]{:T(128)} %get-tuple-element.245), kind=kOutput, calls=%fused_computation.14 | convolution fusion | flops 9108992 | bytes 413700 | tf_op jit(solution)/shard_map/while/body/eval_jaxpr/cond/branch_1_fun/qhd,khd->hqk/dot_general | solution.py:15
  46.9 0.7 dynamic_update_slice.22
  48.9 2.6 %conditional.3 = (f32[1,128,256]{1,2,0:T(8,128)S(1)}, f32[1,4,128]{2,1,0:T(4,128)}) conditional(s32[]{:T(128)} %convert_element_type.82, () %tuple.61, (s32[]{:T(128)}, s32[128]{0:T(128)S(1)}, s32[]{:T(128)}, s32[128]{0:T(128)S(1)}, bf16[4,128,4,64]{1,3,2,0:T(8,128)(2,1)S(1)}, /*index=5*/s32[]{:T(128)}, bf16[128,4,64]{0,2,1:T(8,128)(2,1)S(1)}, ...), branch_computations={%region_2.2_spmd, %region_3.4_spmd} | conditional | flops 119505664 | bytes 1179684 | solution.py:76
  49.0 1.0 %fusion.11 = (f32[4,128]{1,0:T(4,128)}, f32[4,128,128]{1,2,0:T(8,128)S(1)}) fusion(pred[128,128]{0,1:T(8,128)(4,1)S(1)} %broadcast_compare_fusion, f32[4,128]{1,0:T(4,128)S(1)} %convert_bitcast_fusion, bf16[128,4,64]{0,2,1:T(8,128)(2,1)S(1)} %get-tuple-element.246, bf16[4,128,4,64]{1,3,2,0:T(8,128)(2,1)S(1)} %get-tuple-element.244, s32[]{:T(128)} %get-tuple-element.245), kind=kOutput, calls=%fused_computation.14 | convolution fusion | flops 9108992 | bytes 413700 | tf_op jit(solution)/shard_map/while/body/eval_jaxpr/cond/branch_1_fun/qhd,khd->hqk/dot_general | solution.py:15
  53.5 2.6 %conditional.3 = (f32[1,128,256]{1,2,0:T(8,128)S(1)}, f32[1,4,128]{2,1,0:T(4,128)}) conditional(s32[]{:T(128)} %convert_element_type.82, () %tuple.61, (s32[]{:T(128)}, s32[128]{0:T(128)S(1)}, s32[]{:T(128)}, s32[128]{0:T(128)S(1)}, bf16[4,128,4,64]{1,3,2,0:T(8,128)(2,1)S(1)}, /*index=5*/s32[]{:T(128)}, bf16[128,4,64]{0,2,1:T(8,128)(2,1)S(1)}, ...), branch_computations={%region_2.2_spmd, %region_3.4_spmd} | conditional | flops 119505664 | bytes 1179684 | solution.py:76
  53.6 1.0 %fusion.11 = (f32[4,128]{1,0:T(4,128)}, f32[4,128,128]{1,2,0:T(8,128)S(1)}) fusion(pred[128,128]{0,1:T(8,128)(4,1)S(1)} %broadcast_compare_fusion, f32[4,128]{1,0:T(4,128)S(1)} %convert_bitcast_fusion, bf16[128,4,64]{0,2,1:T(8,128)(2,1)S(1)} %get-tuple-element.246, bf16[4,128,4,64]{1,3,2,0:T(8,128)(2,1)S(1)} %get-tuple-element.244, s32[]{:T(128)} %get-tuple-element.245), kind=kOutput, calls=%fused_computation.14 | convolution fusion | flops 9108992 | bytes 413700 | tf_op jit(solution)/shard_map/while/body/eval_jaxpr/cond/branch_1_fun/qhd,khd->hqk/dot_general | solution.py:15
  57.1 13.2 %all_to_all.16 = bf16[4,32,256]{2,1,0:T(8,128)(2,1)S(1)} all-to-all(bf16[4,32,256]{2,1,0:T(8,128)(2,1)S(1)} %bitcast.54), channel_id=1, replica_groups=mesh['grp'=2,'sp'=4,'tp'=4] {'tp'}, dimensions={0} | all-to-all | bytes 131072 | tf_op jit(solution)/shard_map/all_to_all | solution.py:123
  70.3 3.0 %convolution_convert_fusion = bf16[32,2048]{1,0:T(8,128)(2,1)S(1)} fusion(bf16[32,1024]{1,0:T(8,128)(2,1)S(1)} %bitcast.53, bf16[1024,2048]{1,0:T(8,128)(2,1)} %all-gather.2.cloned.1.call-done), kind=kOutput, calls=%fused_computation.32 | convolution fusion | flops 134283264 | bytes 4390912 | tf_op jit(solution)/shard_map/dot_general | solution.py:125
  73.3 7.3 %all_gather.15 = bf16[128,2048]{1,0:T(8,128)(2,1)S(1)} all-gather(bf16[32,2048]{1,0:T(8,128)(2,1)S(1)} %convolution_convert_fusion), channel_id=1, replica_groups=mesh['grp'=2,'sp'=4,'tp'=4] {'tp'}, dimensions={0}, use_global_device_ids=true | all-gather | bytes 655360 | tf_op jit(solution)/shard_map/all_gather | solution.py:126
  80.5 0.8 copy.79
  (77 shorter events, 12.7 us)
Async XLA Ops:
  6.5 2.1 %copy-start = (bf16[2048,256]{1,0:T(8,128)(2,1)S(1)}, bf16[2048,256]{1,0:T(8,128)(2,1)}, u32[]{:S(2)}) copy-start(bf16[2048,256]{1,0:T(8,128)(2,1)} %param.14) | copy-start | bytes 3145732
  6.5 8.4 %copy-start.1 = (bf16[128,2048]{1,0:T(8,128)(2,1)S(1)}, bf16[128,2048]{1,0:T(8,128)(2,1)}, u32[]{:S(2)}) copy-start(bf16[128,2048]{1,0:T(8,128)(2,1)} %param.11) | copy-start | bytes 1572868
  6.5 8.4 %copy-start.4 = (f32[2048]{0:T(1024)S(1)}, f32[2048]{0:T(1024)}, u32[]{:S(2)}) copy-start(f32[2048]{0:T(1024)} %param.12) | copy-start | bytes 24580
  6.5 8.4 %copy-start.3 = (bf16[2048,256]{1,0:T(8,128)(2,1)S(1)}, bf16[2048,256]{1,0:T(8,128)(2,1)}, u32[]{:S(2)}) copy-start(bf16[2048,256]{1,0:T(8,128)(2,1)} %param.13) | copy-start | bytes 3145732
  6.5 63.7 %all-gather.2.cloned.1.call-start = ((), (), s32[]{:S(2)}) async-start(), calls=%async_computation.1 | async-start | bytes 5242880 | tf_op jit(solution)/shard_map/all_gather | solution.py:124
  7.3 24.7 %copy-start.2 = (bf16[4,128]{1,0:T(4,128)(2,1)S(1)}, bf16[4,128]{1,0:T(4,128)(2,1)}, u32[]{:S(2)}) copy-start(bf16[4,128]{1,0:T(4,128)(2,1)} %param.17) | copy-start | bytes 3076
  10.0 3.2 %collective-permute-start = (bf16[128,256]{1,0:T(8,128)(2,1)S(1)}, bf16[128,256]{1,0:T(8,128)(2,1)S(1)}, u32[]{:S(2)}, u32[]{:S(2)}) collective-permute-start(bf16[128,256]{1,0:T(8,128)(2,1)S(1)} %convolution_convert_fusion.3), channel_id=1, source_target_pairs={{0,4},{4,8},{8,12},{12,0},{1,5},{5,9},{9,13},{13,1},{2,6},{6,10},{... | collective-permute-start | bytes 196616 | tf_op jit(solution)/shard_map/ppermute | solution.py:93
  13.2 3.1 %collective-permute-start.1 = (bf16[128,256]{1,0:T(8,128)(2,1)S(1)}, bf16[128,256]{1,0:T(8,128)(2,1)S(1)}, u32[]{:S(2)}, u32[]{:S(2)}) collective-permute-start(bf16[128,256]{1,0:T(8,128)(2,1)S(1)} %collective-permute-done), channel_id=1, source_target_pairs={{0,4},{4,8},{8,12},{12,0},{1,5},{5,9},{9,13},{13,1},{2,6},{6,10},{... | collective-permute-start | bytes 196616 | tf_op jit(solution)/shard_map/ppermute | solution.py:93
  16.3 21.3 %collective-permute-start.2 = (bf16[128,256]{1,0:T(8,128)(2,1)S(1)}, bf16[128,256]{1,0:T(8,128)(2,1)S(1)}, u32[]{:S(2)}, u32[]{:S(2)}) collective-permute-start(bf16[128,256]{1,0:T(8,128)(2,1)S(1)} %collective-permute-done.1), channel_id=1, source_target_pairs={{0,4},{4,8},{8,12},{12,0},{1,5},{5,9},{9,13},{13,1},{2,6},{6,10},{... | collective-permute-start | bytes 196616 | tf_op jit(solution)/shard_map/ppermute | solution.py:93
Sparse Core Ops, SparseCore 0:
  8.9 35.8 all-gather.1
